TPU v7x, 32 devices: a whole 2x2x4 slice. The times are simulated.
32 devices in a mesh: vp: 8 (over z, x), dp: 4 (over y, core).
Axes of the slice: x: 2, y: 2, z: 4, core: 2. Of those that a mesh axis runs over, the one named last changes fastest.
Arguments:
- hidden: bfloat16 [4096, 5632], P(('vp', 'dp')), may hold values from -6 to 6
- down_weight: bfloat16 [5632, 2048], P('vp'), may hold values from -0.078125 to 0.078125
- residual: bfloat16 [4096, 2048], P(('vp', 'dp')), may hold values from -20 to 20
- post_gain: float32 [2048], replicated, may hold values from 0.1 to 1.9
- final_gain: float32 [2048], replicated, may hold values from 0.1 to 1.9
- vocab_matrix: bfloat16 [2048, 32768], P(None, 'vp'), may hold values from -8 to 8
- vocab_bias: float32 [32768], P('vp'), may hold values from -3.5 to 3.5
- targets: int32 [4096], P(('vp', 'dp')), may hold values from 0 to 32767
Outputs:
- losses: float32 [4096], P(('vp', 'dp'))
- norm_grad: float32 [4096, 2048], P(('vp', 'dp'))
- vocab_grad: float32 [2048, 32768], P('dp', 'vp')
All inputs are finite; a program needn't handle non-finite values.
Results may differ from a plain program's by a relative error of at most 0.01.
Values may be sent and summed in bfloat16 or wider, within the bound.
A program may use at most 128 MiB of HBM per device.

v0:
```python
import functools
import math

import jax
import jax.numpy as jnp
from jax import lax
from jax.experimental import pallas as pl
from jax.experimental.pallas import tpu as pltpu
from jax.sharding import PartitionSpec as P


norm_eps = 1e-06
zloss_weight = 0.0001
MESH = pl.DeviceIdType.MESH
f32, bf16 = jnp.float32, jnp.bfloat16


class Place:
    def __init__(self, nx, nz):
        self.nx, self.nz, self.count = nx, nz, nx * nz
        self.vp, self.dp = lax.axis_index("vp"), lax.axis_index("dp")
        self.x, self.z = lax.rem(self.vp, nx), self.vp // nx
        self.other_core = self.dp + 1 - 2 * lax.rem(self.dp, 2)

    def side(self, step):
        return lax.rem(self.x + step, self.nx)

    def at(self, x, z):
        return (z * self.nx + x, self.dp)

    def outward(self, k):
        return jnp.where(lax.rem(k, 2) == 0, k // 2, self.nz - 1 - k // 2)

    def nearby(self, k):
        low, high = self.z, self.nz - 1 - self.z
        both = jnp.minimum(low, high)
        half = (k + 1) // 2
        near = jnp.where(lax.rem(k, 2) == 1, self.z - half, self.z + half)
        far = jnp.where(high > low, self.z + (k - both), self.z - (k - both))
        return jnp.where(k <= 2 * both, near, far)


def arrived(ref, sem):
    pltpu.make_async_copy(ref, ref, sem).wait()


def send(src, dst, send_sem, recv_sem, device):
    pltpu.make_async_remote_copy(
        src_ref=src, dst_ref=dst, send_sem=send_sem, recv_sem=recv_sem,
        device_id=device, device_id_type=MESH,
    ).start()


def greet(place, everyone):
    barrier = pltpu.get_barrier_semaphore()
    for step in range(1, place.count):
        peer = lax.rem(place.vp + step, place.count)
        pl.semaphore_signal(barrier, inc=1, device_id=(peer, place.dp), device_id_type=MESH)
        if everyone:
            pl.semaphore_signal(
                barrier, inc=1, device_id=(peer, place.other_core), device_id_type=MESH
            )
    pl.semaphore_signal(
        barrier, inc=1, device_id=(place.vp, place.other_core), device_id_type=MESH
    )
    pl.semaphore_wait(barrier, place.count + (place.count - 1 if everyone else 0))


def row_loop(rows, size, body):
    @pl.loop(0, rows // size)
    def _(r):
        body(pl.ds(pl.multiple_of(r * size, size), size))


def line_reduce_scatter(place, splits, produce, px, xr, q, sb, zd, zu, sems):
    nx, nz, z = place.nx, place.nz, place.z
    xs_sem, xr_sem, zs_sem, zd_sem, zu_sem = sems
    rows = q.shape[2]
    size = min(rows, 32)

    def add(zb, s, ref):
        def body(r):
            q[zb, s, r] += ref[r].astype(f32)

        row_loop(rows, size, body)

    def pass_on(zb, s):
        def body(r):
            sb[zb, s, r] = q[zb, s, r].astype(bf16)

        row_loop(rows, size, body)

    def below(zb, s):
        @pl.when(z < nz - 1)
        def _():
            arrived(zd.at[zb, s], zd_sem.at[zb, s])
            add(zb, s, zd.at[zb, s])

    def above(zb, s):
        @pl.when(z > 0)
        def _():
            arrived(zu.at[zb, s], zu_sem.at[zb, s])
            add(zb, s, zu.at[zb, s])

    def sides(zb, s):
        for step in range(1, nx):
            arrived(xr.at[step - 1, zb, s], xr_sem.at[step - 1, zb, s])
            add(zb, s, xr.at[step - 1, zb, s])

    @pl.loop(0, nz + 1)
    def _(k):
        @pl.when(k < nz)
        def _():
            zb = place.outward(k)
            produce(zb)
            for s in range(splits):
                for step in range(1, nx):
                    slot = nx - step - 1
                    send(px.at[step - 1, zb, s], xr.at[slot, zb, s], xs_sem.at[step - 1, zb, s],
                         xr_sem.at[slot, zb, s], place.at(place.side(step), z))

        zc = place.outward(jnp.maximum(k - 1, 0))

        @pl.when((k > 0) & (zc < z))
        def _():
            for s in range(splits):
                sides(zc, s)
                below(zc, s)
                pass_on(zc, s)
                send(sb.at[zc, s], zd.at[zc, s], zs_sem.at[zc, s], zd_sem.at[zc, s],
                     place.at(place.x, z - 1))

        @pl.when((k > 0) & (zc > z))
        def _():
            for s in range(splits):
                sides(zc, s)
                above(zc, s)
                pass_on(zc, s)
                send(sb.at[zc, s], zu.at[zc, s], zs_sem.at[zc, s], zu_sem.at[zc, s],
                     place.at(place.x, z + 1))

    for s in range(splits):
        sides(z, s)
        below(z, s)
        above(z, s)

    @pl.loop(0, nz)
    def _(zb):
        for s in range(splits):
            for step in range(1, nx):
                arrived(px.at[step - 1, zb, s], xs_sem.at[step - 1, zb, s])

            @pl.when(zb != z)
            def _():
                arrived(sb.at[zb, s], zs_sem.at[zb, s])


def front_kernel(
    nx, nz, splits,
    hid, weight_in, residual, post_gain, final_gain, targets, vocab, bias,
    normed_out, dlogits_out, stream_out, losses_out,
    units, weight, px, xr, q, sb, zd, zu, normed,
    targets_out, vocab_part, scores, exps, stats, stats_in, total_own, total_in,
    xs_sem, xr_sem, zs_sem, zd_sem, zu_sem,
    hid_send, hid_recv, tgt_send, tgt_recv,
    side_send, line_send, gather_recv, core_send, core_recv, out_sem,
    weight_sem, vocab_sem, stats_send, stats_recv, total_send, total_recv, grad_sem,
):
    place = Place(nx, nz)
    count, vp, z = place.count, place.vp, place.z
    split_rows, width = q.shape[2], q.shape[3]
    rows, lanes = splits * split_rows, targets.shape[1]
    cols = vocab_part.shape[1]
    core = lax.rem(place.dp, 2)
    tile = min(cols, 512)
    vocab_load = pltpu.make_async_copy(
        vocab.at[:, pl.ds(pl.multiple_of(core * cols, cols), cols)], vocab_part, vocab_sem
    )
    weight_load = pltpu.make_async_copy(weight_in, weight, weight_sem)
    weight_load.start()
    greet(place, True)

    own = pltpu.make_async_copy(hid.at[vp], units.at[vp], hid_recv.at[vp])
    own.start()
    for k in range(count - 1):
        peer = lax.rem(vp + k + 1, count)
        send(hid.at[peer], units.at[vp], hid_send.at[k], hid_recv.at[vp], (peer, place.dp))
    for k in range(count - 1):
        peer = lax.rem(vp + k + 1, count)
        for c in range(2):
            send(targets, targets_out.at[c, vp], tgt_send.at[c, k], tgt_recv.at[c, vp],
                 (peer, place.other_core if c else place.dp))
    send(targets, targets_out.at[1, vp], tgt_send.at[1, count - 1], tgt_recv.at[1, vp],
         (vp, place.other_core))
    own_targets = pltpu.make_async_copy(targets, targets_out.at[0, vp], tgt_recv.at[0, vp])
    own_targets.start()
    vocab_load.start()
    weight_load.wait()

    def product(device, store):
        arrived(units.at[device], hid_recv.at[device])
        tile = min(width, 512)

        @pl.loop(0, width // tile)
        def _(n):
            cols = pl.ds(pl.multiple_of(n * tile, tile), tile)
            store(cols, jnp.dot(units[device], weight[:, cols], preferred_element_type=f32))

    def produce(zb):
        for step in range(nx):
            def store(cols, value):
                for s in range(splits):
                    part = value[s * split_rows : (s + 1) * split_rows]
                    if step == 0:
                        q[zb, s, :, cols] = part
                    else:
                        px[step - 1, zb, s, :, cols] = part.astype(bf16)

            product(zb * nx + place.side(step), store)

    line_reduce_scatter(
        place, splits, produce, px, xr, q, sb, zd, zu, (xs_sem, xr_sem, zs_sem, zd_sem, zu_sem)
    )

    for s in range(splits):
        def norms(r):
            mixed = q[z, s, r]
            post = mixed * lax.rsqrt(jnp.mean(mixed * mixed, axis=-1, keepdims=True) + norm_eps)
            stream = (residual[s, r].astype(f32) + post * post_gain[...]).astype(bf16)
            stream_out[s, r] = stream
            stream = stream.astype(f32)
            inverse = lax.rsqrt(jnp.mean(stream * stream, axis=-1, keepdims=True) + norm_eps)
            normed[0, vp, s, r] = (stream * inverse * final_gain[...]).astype(bf16)

        row_loop(split_rows, 16, norms)

    blocks, block_width = normed_out.shape[0], normed_out.shape[-1]
    plane = place.dp // 2

    def keep(c, i, s):
        for b in range(blocks):
            there = lax.rem(plane + b // 2, blocks // 2)
            at = (there * 2 + lax.rem(core + b, 2)) * block_width
            pltpu.make_async_copy(
                normed.at[c, i, s, :, pl.ds(pl.multiple_of(at, block_width), block_width)],
                normed_out.at[b, c, i, s], out_sem.at[c, i, s],
            ).start()

    def to_core(i, s):
        keep(0, i, s)
        send(normed.at[0, i, s], normed.at[1, i, s], core_send.at[i, s], core_recv.at[i, s],
             (vp, place.other_core))

    @pl.loop(0, count)
    def _(i):
        for c in range(2):
            arrived(targets_out.at[c, i], tgt_recv.at[c, i])

    vocab_load.wait()
    first_column = vp * 2 * cols + core * cols

    def column_of(row):
        return jnp.transpose(jnp.broadcast_to(row, (128, lanes)))[:rows, :1]

    def row_of(column):
        return jnp.transpose(jnp.broadcast_to(column, (rows, 128)))[:1, :]

    def score(i):
        for s in range(splits):
            arrived(normed.at[1, i, s], core_recv.at[i, s])
            keep(1, i, s)
        block = jnp.concatenate(
            [normed[c, i, s] for c in range(2) for s in range(splits)], axis=0
        )
        high = jnp.full((2 * rows, 1), -jnp.inf, f32)
        for n in range(cols // tile):
            at = slice(n * tile, (n + 1) * tile)
            value = jnp.dot(block, vocab_part[:, at], preferred_element_type=f32) + bias[:, at]
            scores[:, at] = value
            high = jnp.maximum(high, jnp.max(value, axis=1, keepdims=True))
        for c in range(2):
            part = slice(c * rows, (c + 1) * rows)
            target = column_of(targets_out[c, i]) - first_column
            top = high[part]
            total = jnp.zeros((rows, 1), f32)
            picked = jnp.zeros((rows, 1), f32)
            for n in range(cols // tile):
                at = slice(n * tile, (n + 1) * tile)
                value = scores[part, at]
                ids = n * tile + lax.broadcasted_iota(jnp.int32, (rows, tile), 1)
                raised = jnp.exp(value - top)
                total += jnp.sum(raised, axis=1, keepdims=True)
                picked += jnp.sum(jnp.where(ids == target, value, 0.0), axis=1, keepdims=True)
                exps[c, i, :, at] = raised.astype(bf16)
            for j, value in enumerate((top, total, picked)):
                stats[c, i, j : j + 1, :rows] = row_of(value)

        @pl.when(i != vp)
        def _():
            for c in range(2):
                send(stats.at[c, i], stats_in.at[c, vp], stats_send.at[c, i], stats_recv.at[c, vp],
                     (i, place.other_core if c else place.dp))

        @pl.when(i == vp)
        def _():
            send(stats.at[1, i], stats_in.at[1, vp], stats_send.at[1, i], stats_recv.at[1, vp],
                 (vp, place.other_core))
            pltpu.make_async_copy(stats.at[0, i], stats_in.at[0, vp], stats_recv.at[0, vp]).start()

    @pl.loop(0, nz + 1)
    def _(k):
        @pl.when(k < nz)
        def _():
            zb = place.nearby(k)
            i = zb * nx + place.x
            for s in range(splits):
                block, sem = normed.at[0, i, s], gather_recv.at[i, s]

                @pl.when(k > 0)
                def _():
                    arrived(block, sem)

                @pl.when((zb >= z) & (z > 0))
                def _():
                    send(block, block, line_send.at[0, zb, s], sem, place.at(place.x, z - 1))

                @pl.when((zb <= z) & (z < nz - 1))
                def _():
                    send(block, block, line_send.at[1, zb, s], sem, place.at(place.x, z + 1))

                for step in range(1, nx):
                    send(block, block, side_send.at[step - 1, zb, s], sem,
                         place.at(place.side(step), z))
                to_core(i, s)

        @pl.when(k > 0)
        def _():
            zb = place.nearby(k - 1)
            for step in range(1, nx):
                i = zb * nx + place.side(step)
                for s in range(splits):
                    arrived(normed.at[0, i, s], gather_recv.at[i, s])
                    to_core(i, s)

        @pl.loop(0, nx)
        def _(step):
            @pl.when(((step == 0) & (k < nz)) | ((step > 0) & (k > 0)))
            def _():
                zb = place.nearby(jnp.where(step == 0, jnp.minimum(k, nz - 1), jnp.maximum(k - 1, 0)))
                score(zb * nx + place.side(step))

    @pl.loop(0, count)
    def _(i):
        for c in range(2):
            arrived(stats_in.at[c, i], stats_recv.at[c, i])

    pairs = [(c, i) for c in range(2) for i in range(count)]
    top = stats_in[0, 0, 0:1]
    for c, i in pairs[1:]:
        top = jnp.maximum(top, stats_in[c, i, 0:1])
    total = jnp.zeros((1, lanes), f32)
    picked = jnp.zeros((1, lanes), f32)
    for c, i in pairs:
        total += stats_in[c, i, 1:2] * jnp.exp(stats_in[c, i, 0:1] - top)
        picked += stats_in[c, i, 2:3]
    log_total = top + jnp.log(total)
    total_own[...] = log_total
    losses_out[...] = log_total - picked + zloss_weight * log_total * log_total
    for k in range(count - 1):
        peer = lax.rem(vp + k + 1, count)
        for c in range(2):
            send(total_own, total_in.at[c, vp], total_send.at[c, k], total_recv.at[c, vp],
                 (peer, place.other_core if c else place.dp))
    send(total_own, total_in.at[1, vp], total_send.at[1, count - 1], total_recv.at[1, vp],
         (vp, place.other_core))
    pltpu.make_async_copy(total_own, total_in.at[0, vp], total_recv.at[0, vp]).start()

    @pl.loop(0, count)
    def _(k):
        i = lax.rem(vp + k, count)
        for c in range(2):
            arrived(total_in.at[c, i], total_recv.at[c, i])
            log_total = total_in[c, i]
            factor = jnp.exp(stats[c, i, 0:1] - log_total) * (1.0 + 2.0 * zloss_weight * log_total)
            factor = column_of(factor)
            target = column_of(targets_out[c, i]) - first_column
            for n in range(cols // tile):
                at = slice(n * tile, (n + 1) * tile)
                ids = n * tile + lax.broadcasted_iota(jnp.int32, (rows, tile), 1)
                value = exps[c, i, :, at].astype(f32) * factor - jnp.where(ids == target, 1.0, 0.0)
                exps[c, i, :, at] = value.astype(bf16)
            pltpu.make_async_copy(exps.at[c, i], dlogits_out.at[c, i], grad_sem.at[c, i]).start()

    @pl.loop(0, nz)
    def _(zb):
        for s in range(splits):
            block = normed.at[0, zb * nx + place.x, s]

            @pl.when((zb >= z) & (z > 0))
            def _():
                arrived(block, line_send.at[0, zb, s])

            @pl.when((zb <= z) & (z < nz - 1))
            def _():
                arrived(block, line_send.at[1, zb, s])

            for step in range(1, nx):
                arrived(block, side_send.at[step - 1, zb, s])

    @pl.loop(0, count)
    def _(i):
        for s in range(splits):
            arrived(normed.at[0, i, s], core_send.at[i, s])
            for c in range(2):
                arrived(normed.at[c, i, s], out_sem.at[c, i, s])

    @pl.loop(0, count)
    def _(i):
        for c in range(2):
            arrived(exps.at[c, i], grad_sem.at[c, i])
        arrived(stats.at[1, i], stats_send.at[1, i])

        @pl.when(i != vp)
        def _():
            arrived(stats.at[0, i], stats_send.at[0, i])

    for k in range(count - 1):
        arrived(hid.at[0], hid_send.at[k])
        for c in range(2):
            arrived(targets, tgt_send.at[c, k])
            arrived(total_own, total_send.at[c, k])
    arrived(targets, tgt_send.at[1, count - 1])
    arrived(total_own, total_send.at[1, count - 1])


def rs_scratch(nx, nz, splits, rows, width):
    shape = (nz, splits, rows, width)
    return [
        pltpu.VMEM((nx - 1,) + shape, bf16),
        pltpu.VMEM((nx - 1,) + shape, bf16),
        pltpu.VMEM(shape, f32),
        pltpu.VMEM(shape, bf16),
        pltpu.VMEM(shape, bf16),
        pltpu.VMEM(shape, bf16),
    ]


def rs_sems(nx, nz, splits):
    dma = pltpu.SemaphoreType.DMA
    return [dma((nx - 1, nz, splits))] * 2 + [dma((nz, splits))] * 3


def front(nx, nz, splits, blocks, hid, weight, residual, post_gain, final_gain, targets, vocab, bias):
    count, rows, _ = hid.shape
    width = weight.shape[1]
    split_rows = rows // splits
    dma = pltpu.SemaphoreType.DMA
    vmem = pl.BlockSpec(memory_space=pltpu.VMEM)
    hbm = pl.BlockSpec(memory_space=pl.ANY)
    cols, lanes = bias.shape[1], targets.shape[1]
    flops = 2 * count * rows * weight.shape[0] * width
    return pl.pallas_call(
        functools.partial(front_kernel, nx, nz, splits),
        out_shape=(
            jax.ShapeDtypeStruct((blocks, 2, count, splits, split_rows, width // blocks), bf16),
            jax.ShapeDtypeStruct((2, count, rows, cols), bf16),
            jax.ShapeDtypeStruct((splits, split_rows, width), bf16),
            jax.ShapeDtypeStruct((1, lanes), f32),
        ),
        in_specs=[hbm] * 2 + [vmem] * 4 + [hbm, vmem],
        out_specs=(hbm, hbm, vmem, vmem),
        scratch_shapes=[pltpu.VMEM(hid.shape, bf16), pltpu.VMEM(weight.shape, bf16)]
        + rs_scratch(nx, nz, splits, split_rows, width)
        + [
            pltpu.VMEM((2, count, splits, split_rows, width), bf16),
            pltpu.VMEM((2, count, 1, lanes), jnp.int32),
            pltpu.VMEM((width, cols), bf16),
            pltpu.VMEM((2 * rows, cols), f32),
            pltpu.VMEM((2, count, rows, cols), bf16),
            pltpu.VMEM((2, count, 8, lanes), f32),
            pltpu.VMEM((2, count, 8, lanes), f32),
            pltpu.VMEM((1, lanes), f32),
            pltpu.VMEM((2, count, 1, lanes), f32),
        ]
        + rs_sems(nx, nz, splits)
        + [
            dma((count - 1,)), dma((count,)), dma((2, count)), dma((2, count)),
            dma((nx - 1, nz, splits)), dma((2, nz, splits)), dma((count, splits)),
            dma((count, splits)), dma((count, splits)), dma((2, count, splits)),
            dma, dma, dma((2, count)), dma((2, count)), dma((2, count)), dma((2, count)),
            dma((2, count)),
        ],
        compiler_params=pltpu.CompilerParams(
            collective_id=0, has_side_effects=True, vmem_limit_bytes=60 << 20
        ),
        cost_estimate=pl.CostEstimate(flops=flops, bytes_accessed=1 << 24, transcendentals=0),
        name="front",
    )(hid, weight, residual.reshape(splits, split_rows, width), post_gain, final_gain, targets,
      vocab, bias)


def back_kernel(
    nx, nz, splits,
    dlogits, vocab, own_out,
    grads, vocab_part, terms, given, theirs, px, xr, q, sb, zd, zu,
    xs_sem, xr_sem, zs_sem, zd_sem, zu_sem,
    load_sem, vocab_sem, core_send, core_recv,
):
    place = Place(nx, nz)
    count, z = place.count, place.z
    split_rows = q.shape[2]
    rows = splits * split_rows
    cols = vocab_part.shape[2]
    pieces, piece = vocab_part.shape[0], vocab_part.shape[1]
    core = lax.rem(place.dp, 2)
    greet(place, False)

    def load(zb):
        for step in range(nx):
            i = zb * nx + place.side(step)
            for c in range(2):
                pltpu.make_async_copy(dlogits.at[c, i], grads.at[c, i], load_sem.at[c, i]).start()

    load(0)
    for n in range(pieces):
        pltpu.make_async_copy(
            vocab.at[n * piece : (n + 1) * piece, pl.ds(pl.multiple_of(core * cols, cols), cols)],
            vocab_part.at[n], vocab_sem.at[n],
        ).start()

    @pl.loop(1, nz)
    def _(k):
        load(place.outward(k))

    def produce(zb):
        for step in range(nx):
            i = zb * nx + place.side(step)
            for c in range(2):
                arrived(grads.at[c, i], load_sem.at[c, i])
            block = jnp.concatenate([grads[0, i], grads[1, i]], axis=0)

            @pl.loop(0, pieces)
            def _(n):
                if step == 0:
                    @pl.when(zb == 0)
                    def _():
                        arrived(vocab_part.at[n], vocab_sem.at[n])

                at = pl.ds(pl.multiple_of(n * piece, piece), piece)
                value = lax.dot_general(
                    block, vocab_part[n], (((1,), (1,)), ((), ())), preferred_element_type=f32
                )
                for s in range(splits):
                    r = s * split_rows
                    terms[step, s, :, at] = value[r : r + split_rows]
                    given[i, s, :, at] = value[rows + r : rows + r + split_rows].astype(bf16)

            for s in range(splits):
                send(given.at[i, s], theirs.at[i, s], core_send.at[i, s], core_recv.at[i, s],
                     (place.vp, place.other_core))
        for step in range(nx):
            i = zb * nx + place.side(step)
            for s in range(splits):
                arrived(theirs.at[i, s], core_recv.at[i, s])

                def body(r):
                    value = terms[step, s, r] + theirs[i, s, r].astype(f32)
                    if step == 0:
                        q[zb, s, r] = value
                    else:
                        px[step - 1, zb, s, r] = value.astype(bf16)

                row_loop(split_rows, 16, body)

    line_reduce_scatter(
        place, splits, produce, px, xr, q, sb, zd, zu, (xs_sem, xr_sem, zs_sem, zd_sem, zu_sem)
    )
    for s in range(splits):
        def body(r):
            own_out[s, r] = q[z, s, r]

        row_loop(split_rows, 16, body)

    @pl.loop(0, count)
    def _(i):
        for s in range(splits):
            arrived(given.at[i, s], core_send.at[i, s])


def back(nx, nz, splits, dlogits, vocab):
    _, count, rows, cols = dlogits.shape
    width = vocab.shape[0]
    split_rows = rows // splits
    piece = math.gcd(width, 512)
    dma = pltpu.SemaphoreType.DMA
    shape = (count, splits, split_rows, width)
    hbm = pl.BlockSpec(memory_space=pl.ANY)
    return pl.pallas_call(
        functools.partial(back_kernel, nx, nz, splits),
        out_shape=jax.ShapeDtypeStruct((splits, split_rows, width), f32),
        in_specs=[hbm, hbm],
        out_specs=pl.BlockSpec(memory_space=pltpu.VMEM),
        scratch_shapes=[
            pltpu.VMEM((2, count, rows, cols), bf16),
            pltpu.VMEM((width // piece, piece, cols), bf16),
            pltpu.VMEM((nx, splits, split_rows, width), f32),
            pltpu.VMEM(shape, bf16),
            pltpu.VMEM(shape, bf16),
        ]
        + rs_scratch(nx, nz, splits, split_rows, width)
        + rs_sems(nx, nz, splits)
        + [dma((2, count)), dma((width // piece,)), dma((count, splits)), dma((count, splits))],
        compiler_params=pltpu.CompilerParams(
            collective_id=1, has_side_effects=True, vmem_limit_bytes=56 << 20
        ),
        cost_estimate=pl.CostEstimate(
            flops=4 * count * rows * cols * width, bytes_accessed=1 << 24, transcendentals=0
        ),
        name="back",
    )(dlogits, vocab)


def on_device(
    nx, nz, hidden, down_weight, residual, post_gain, final_gain, vocab_matrix, vocab_bias, targets
):
    rows, width = residual.shape
    count = lax.axis_size("vp")
    dp_size = lax.axis_size("dp")
    planes = dp_size // 2
    splits = 4 if rows % 64 == 0 else 2 if rows % 32 == 0 else 1
    core = lax.axis_index("dp") % 2
    units = hidden.reshape(rows, count, hidden.shape[1] // count).transpose(1, 0, 2)
    lanes = -(-rows // 128) * 128
    padded = jnp.pad(targets, (0, lanes - rows)).reshape(1, lanes)
    cols = vocab_matrix.shape[1] // 2
    bias_half = lax.dynamic_slice_in_dim(vocab_bias, core * cols, cols, 0)
    normed, dlogits, stream, losses = front(
        nx, nz, splits, 2 * planes, units, down_weight, residual,
        post_gain.reshape(1, -1), final_gain.reshape(1, -1), padded,
        vocab_matrix, bias_half.reshape(1, -1),
    )
    stream = stream.reshape(rows, width)
    tokens = 2 * count * rows
    token_rows = normed.reshape(2 * planes, tokens, width // (2 * planes))
    dlogits_2d = dlogits.reshape(tokens, cols)

    core_pairs = [(d, d ^ 1) for d in range(dp_size)]
    spans = column_spans(cols)
    arrivals = []
    source = dlogits_2d
    for low, high in spans:
        got = []
        for shift in range(1, planes):
            for c in range(2):
                grads = lax.dot_general(
                    token_rows[2 * shift + c], source[:, low:high],
                    (((0,), (0,)), ((), ())), preferred_element_type=f32,
                ).astype(bf16)
                grads, source = lax.optimization_barrier((grads, source))
                to = [
                    (d, ((d // 2 + shift) % planes) * 2 + (d % 2 + c) % 2) for d in range(dp_size)
                ]
                got.append(lax.ppermute(grads, "dp", to))
        arrivals.append(got)
    dnormed = back(nx, nz, splits, source.reshape(dlogits.shape), vocab_matrix)
    dnormed, source = lax.optimization_barrier((dnormed, source))
    dnormed = dnormed.reshape(rows, width)
    halves = [
        lax.dot_general(
            token_rows[c], source, (((0,), (0,)), ((), ())), preferred_element_type=f32,
        )
        for c in (1, 0)
    ]
    given = lax.ppermute(halves[0].astype(bf16), "dp", core_pairs)
    kept = halves[1]

    def total(c, base):
        parts = [
            sum(arrivals[k][2 * j + c].astype(f32) for j in range(planes - 1))
            for k in range(len(spans))
        ]
        return base.astype(f32) + jnp.concatenate(parts, axis=1)

    same, cross = total(0, kept), total(1, given)
    vocab_grad = jnp.concatenate(
        [jnp.where(core == 0, same, cross), jnp.where(core == 0, cross, same)], axis=1
    )
    stream_f = stream.astype(f32)
    inverse = lax.rsqrt(jnp.mean(stream_f * stream_f, axis=-1, keepdims=True) + norm_eps)
    scaled = stream_f * inverse
    dscaled = dnormed * final_gain[None, :]
    norm_grad = inverse * (dscaled - scaled * jnp.mean(dscaled * scaled, axis=-1, keepdims=True))
    return (losses[0, :rows], norm_grad, vocab_grad)


def column_spans(cols):
    first = 512
    return ((0, first), (first, cols)) if cols > first else ((0, cols),)


def solution(mesh):
    count = mesh.shape["vp"]
    nx = math.isqrt(count // 2)
    nx = nx if nx > 1 and count % nx == 0 else 2
    placed = (
        P(("vp", "dp"), None), P("vp", None), P(("vp", "dp"), None), P(), P(),
        P(None, "vp"), P("vp"), P(("vp", "dp")),
    )
    return jax.shard_map(
        functools.partial(on_device, nx, count // nx),
        mesh=mesh,
        in_specs=placed,
        out_specs=(P(("vp", "dp")), P(("vp", "dp"), None), P("dp", "vp")),
        check_vma=False,
    )
```

profile of v0, /device:TPU:11, one launch (start us, length us, event | category | flops | bytes accessed | tf_op | source)
XLA Modules:
  0.0 381.2 jit_solution(11647535915273355364)
XLA Ops:
  0.6 1.8 copy.11
  2.5 0.0 copy-start.4
  2.5 1.6 copy.12
  4.1 0.0 copy-done.4
  4.1 0.6 dynamic_slice.3
  4.7 159.3 %front.1 = (bf16[4,2,8,4,32,512]{5,4,3,2,1,0:T(8,128)(2,1)}, bf16[2,8,128,2048]{3,2,1,0:T(8,128)(2,1)}, bf16[4,32,2048]{2,1,0:T(8,128)(2,1)}, f32[1,128]{1,0:T(1,128)}) custom-call(bf16[8,128,704]{2,1,0:T(8,128)(2,1)} %bitcast.34, bf16[704,2048]{1,0:T(8,128)(2,1)} %weight_in.1, bf16[4,32,2048]{2,1,0:T(8,128)(2,1)} %bitcast.42, f32[1,2048]{1,0:T(1,128)} %bitcast.45, ...), custom_call_target="tpu_custom_call" | custom-call | flops 2952790016 | bytes 16777216 | tf_op jit(solution)/shard_map/front/pallas_call | solution.py:462
  163.9 0.0 copy-start.5
  164.0 5.0 %fusion.25 = (bf16[1,2,8,4,32,512]{5,4,3,2,1,0:T(8,128)(2,1)}, bf16[1,2,8,4,32,512]{5,4,3,2,1,0:T(8,128)(2,1)S(1)}, bf16[1,2,8,4,32,512]{5,4,3,2,1,0:T(8,128)(2,1)S(1)}, bf16[1,2,8,4,32,512]{5,4,3,2,1,0:T(8,128)(2,1)S(1)}) fusion(bf16[4,2,8,4,32,512]{5,4,3,2,1,0:T(8,128)(2,1)} %get-tuple-element.19), kind=kLoop, calls=%fused_computation.29 | loop fusion | bytes 16777216 | tf_op jit(solution)/shard_map/slice | solution.py:670
  168.9 1.6 copy-done.5
  170.6 2.1 fusion.19
  172.6 2.1 fusion.16
  174.7 4.7 %fusion.6 = bf16[512,1536]{1,0:T(8,128)(2,1)} fusion(bf16[2048,512]{1,0:T(8,128)(2,1)S(1)} %bitcast.41, bf16[2048,2048]{1,0:T(8,128)(2,1)S(1)} %bitcast.51), kind=kOutput, calls=%fused_computation.9 | convolution fusion | flops 3222011904 | bytes 9961472 | tf_op jit(solution)/shard_map/dot_general | solution.py:655
  179.4 4.7 %fusion.9 = bf16[512,1536]{1,0:T(8,128)(2,1)} fusion(bf16[2048,512]{1,0:T(8,128)(2,1)S(1)} %bitcast.39, bf16[2048,2048]{1,0:T(8,128)(2,1)S(1)} %bitcast.52), kind=kOutput, calls=%fused_computation.10 | convolution fusion | flops 3222011904 | bytes 9961472 | tf_op jit(solution)/shard_map/dot_general | solution.py:655
  184.1 80.2 %back.1 = f32[4,32,2048]{2,1,0:T(8,128)} custom-call(bf16[2,8,128,2048]{3,2,1,0:T(8,128)(2,1)} %get-tuple-element.20, bf16[2048,4096]{1,0:T(8,128)(2,1)} %vocab.3), custom_call_target="tpu_custom_call" | custom-call | flops 17179869184 | bytes 16777216 | tf_op jit(solution)/shard_map/back/pallas_call | solution.py:598
  264.3 0.0 copy-start
  264.3 0.0 copy-start.1
  264.3 0.0 copy-start.3
  264.3 9.3 %convolution_convert_fusion = bf16[512,2048]{1,0:T(8,128)(2,1)} fusion(bf16[2048,512]{1,0:T(8,128)(2,1)S(1)} %bitcast.37, bf16[2048,2048]{1,0:T(8,128)(2,1)} %bitcast.47), kind=kOutput, calls=%fused_computation.11 | convolution fusion | flops 4296015872 | bytes 12582912 | tf_op jit(solution)/shard_map/dot_general | solution.py:669
  273.6 1.7 collective-permute-start.2
  275.2 1.1 collective-permute-start.4
  276.3 0.2 collective-permute-start.1
  276.6 1.9 collective-permute-start.3
  278.5 0.2 collective-permute-start
  278.7 0.0 copy-done
  278.7 0.2 multiply_reduce_fusion.1
  278.9 0.0 copy-done.1
  278.9 0.0 copy-done.3
  278.9 0.3 multiply_reduce_fusion
  279.2 0.1 rsqrt.13
  279.3 0.1 div.10
  279.4 0.0 copy-start.2
  279.4 1.3 fusion.24
  280.7 76.5 %collective-permute-done.3 = bf16[512,512]{1,0:T(8,128)(2,1)} collective-permute-done((bf16[512,512]{1,0:T(8,128)(2,1)}, bf16[512,512]{1,0:T(8,128)(2,1)}, u32[]{:S(2)}, u32[]{:S(2)}) %collective-permute-start.3) | collective-permute-done | bytes 524320 | tf_op jit(solution)/shard_map/ppermute | solution.py:663
  357.2 10.2 %collective-permute-done = bf16[512,512]{1,0:T(8,128)(2,1)} collective-permute-done((bf16[512,512]{1,0:T(8,128)(2,1)}, bf16[512,512]{1,0:T(8,128)(2,1)}, u32[]{:S(2)}, u32[]{:S(2)}) %collective-permute-start) | collective-permute-done | bytes 524320 | tf_op jit(solution)/shard_map/ppermute | solution.py:663
  367.3 0.0 collective-permute-done.4
  367.3 0.0 collective-permute-done.1
  367.3 0.0 collective-permute-done.2
  367.3 0.0 copy-done.2
  367.3 9.4 %fusion.5 = (f32[512,2048]{1,0:T(8,128)S(1)}, f32[512,2048]{1,0:T(8,128)S(1)}) fusion(bf16[512,2048]{1,0:T(8,128)(2,1)} %collective-permute-done.2, pred[]{:T(512)S(6)} %eq.6, bf16[512,1536]{1,0:T(8,128)(2,1)S(1)} %collective-permute-done.4, bf16[512,512]{1,0:T(8,128)(2,1)} %collective-permute-done.3, bf16[512,1536]{1,0:T(8,128)(2,1)} %collective-permute-done.1, ...), kind=kOutput, calls=%fused_computation.8 | convolution fusion | flops 4308598784 | bytes 25165824 | tf_op jit(solution)/shard_map/dot_general | solution.py:669
  376.7 0.0 copy-start.6
  376.7 3.9 %pad_maximum_fusion = f32[512,4096]{1,0:T(8,128)} fusion(f32[512,2048]{1,0:T(8,128)S(1)} %get-tuple-element.32, f32[512,2048]{1,0:T(8,128)S(1)} %get-tuple-element.31), kind=kLoop, calls=%fused_computation | loop fusion | flops 2097152 | bytes 16777216 | tf_op jit(solution)/shard_map/concatenate | solution.py:685
  380.7 0.0 copy-done.6
  380.7 0.5 copy.14
  (2 shorter events, 0.0 us)
Async XLA Ops:
  2.5 1.6 copy-start.4
  163.9 6.6 %copy-start.5 = (bf16[2,8,128,2048]{3,2,1,0:T(8,128)(2,1)S(1)}, bf16[2,8,128,2048]{3,2,1,0:T(8,128)(2,1)}, u32[]{:S(2)}) copy-start(bf16[2,8,128,2048]{3,2,1,0:T(8,128)(2,1)} %get-tuple-element.20) | copy-start | bytes 25165828
  264.3 14.4 %copy-start = (bf16[4,32,2048]{2,1,0:T(8,128)(2,1)S(1)}, bf16[4,32,2048]{2,1,0:T(8,128)(2,1)}, u32[]{:S(2)}) copy-start(bf16[4,32,2048]{2,1,0:T(8,128)(2,1)} %get-tuple-element.18) | copy-start | bytes 1572868
  264.3 14.6 %copy-start.1 = (f32[4,32,2048]{2,1,0:T(8,128)S(1)}, f32[4,32,2048]{2,1,0:T(8,128)}, u32[]{:S(2)}) copy-start(f32[4,32,2048]{2,1,0:T(8,128)} %back.1) | copy-start | bytes 3145732
  264.3 14.6 %copy-start.3 = (f32[2048]{0:T(1024)S(1)}, f32[2048]{0:T(1024)}, u32[]{:S(2)}) copy-start(f32[2048]{0:T(1024)} %param.12) | copy-start | bytes 24580
  273.6 93.8 %collective-permute-start.2 = (bf16[512,2048]{1,0:T(8,128)(2,1)}, bf16[512,2048]{1,0:T(8,128)(2,1)}, u32[]{:S(2)}, u32[]{:S(2)}) collective-permute-start(bf16[512,2048]{1,0:T(8,128)(2,1)} %convolution_convert_fusion), channel_id=1, source_target_pairs={{0,1},{1,0},{2,3},{3,2},{4,5},{5,4},{6,7},{7,6},{8,9},{9,8},{10,11... | collective-permute-start | bytes 6291464 | tf_op jit(solution)/shard_map/ppermute | solution.py:674
  275.2 92.1 %collective-permute-start.4 = (bf16[512,1536]{1,0:T(8,128)(2,1)}, bf16[512,1536]{1,0:T(8,128)(2,1)S(1)}, u32[]{:S(2)}, u32[]{:S(2)}) collective-permute-start(bf16[512,1536]{1,0:T(8,128)(2,1)} %fusion.9), channel_id=1, source_target_pairs={{0,3},{1,2},{2,1},{3,0},{4,7},{5,6},{6,5},{7,4},{8,11},{9,10},{10,... | collective-permute-start | bytes 4718600 | tf_op jit(solution)/shard_map/ppermute | solution.py:663
  276.3 91.0 %collective-permute-start.1 = (bf16[512,1536]{1,0:T(8,128)(2,1)}, bf16[512,1536]{1,0:T(8,128)(2,1)}, u32[]{:S(2)}, u32[]{:S(2)}) collective-permute-start(bf16[512,1536]{1,0:T(8,128)(2,1)} %fusion.6), channel_id=1, source_target_pairs={{0,2},{1,3},{2,0},{3,1},{4,6},{5,7},{6,4},{7,5},{8,10},{9,11},{10,... | collective-permute-start | bytes 4718600 | tf_op jit(solution)/shard_map/ppermute | solution.py:663
  276.6 80.6 %collective-permute-start.3 = (bf16[512,512]{1,0:T(8,128)(2,1)}, bf16[512,512]{1,0:T(8,128)(2,1)}, u32[]{:S(2)}, u32[]{:S(2)}) collective-permute-start(bf16[512,512]{1,0:T(8,128)(2,1)} %fusion.16), channel_id=1, source_target_pairs={{0,3},{1,2},{2,1},{3,0},{4,7},{5,6},{6,5},{7,4},{8,11},{9,10},{10,... | collective-permute-start | bytes 1572872 | tf_op jit(solution)/shard_map/ppermute | solution.py:663
  278.5 88.8 %collective-permute-start = (bf16[512,512]{1,0:T(8,128)(2,1)}, bf16[512,512]{1,0:T(8,128)(2,1)}, u32[]{:S(2)}, u32[]{:S(2)}) collective-permute-start(bf16[512,512]{1,0:T(8,128)(2,1)} %fusion.19), channel_id=1, source_target_pairs={{0,2},{1,3},{2,0},{3,1},{4,6},{5,7},{6,4},{7,5},{8,10},{9,11},{10,... | collective-permute-start | bytes 1572872 | tf_op jit(solution)/shard_map/ppermute | solution.py:663
  279.4 87.9 %copy-start.2 = (bf16[1,2,8,4,32,512]{5,4,3,2,1,0:T(8,128)(2,1)S(1)}, bf16[1,2,8,4,32,512]{5,4,3,2,1,0:T(8,128)(2,1)}, u32[]{:S(2)}) copy-start(bf16[1,2,8,4,32,512]{5,4,3,2,1,0:T(8,128)(2,1)} %get-tuple-element.33) | copy-start | bytes 6291460
  376.7 4.0 %copy-start.6 = (f32[1,128]{1,0:T(1,128)S(1)}, f32[1,128]{1,0:T(1,128)}, u32[]{:S(2)}) copy-start(f32[1,128]{1,0:T(1,128)} %get-tuple-element.17) | copy-start | bytes 1540
where the time goes:
time: 382 us; the launch traced here: 381 us
  Pallas kernels  239 us (63%)
  waiting for transfers between devices  86.6 us (23%)
  matrix products  32.2 us (8%)
  local copies, waits for them, and re-layouts  11.3 us (3%)
  other arithmetic  5.75 us (2%)
  starting transfers between devices  5.14 us (1%)
    pallas_call x1, Pallas kernels, front(): pl.pallas_call(functools.partial(front_kernel, nx, nz, splits), out_shape...  159 us
    ppermute x4, waiting for transfers between devices, on_device(): got.append(lax.ppermute(grads, 'dp', to))  86.6 us
    pallas_call x1, Pallas kernels, back(): pl.pallas_call(functools.partial(back_kernel, nx, nz, splits), out_shape=...  80.2 us
    dot_general x2, matrix products, on_device(): lax.dot_general(token_rows[c], source, (((0,), (0,)), ((), ())), preferre...  18.7 us
    dot_general x4, matrix products, on_device(): lax.dot_general(token_rows[2 * shift + c], source[:, low:high], (((0,), (...  13.5 us
  transfers between devices with their start and end apart: 5, of which 2 were waited for; matrix products, arithmetic and copies ran while one was open for 1% of the time, Pallas kernels for 0%

commit v1 on v0

--- a/solution.py
+++ b/solution.py
@@ -72,7 +72,7 @@
         body(pl.ds(pl.multiple_of(r * size, size), size))
 
 
-def line_reduce_scatter(place, splits, produce, px, xr, q, sb, zd, zu, sems):
+def line_reduce_scatter(place, splits, produce, px, xr, q, sb, zd, zu, sems, meanwhile=None):
     nx, nz, z = place.nx, place.nz, place.z
     xs_sem, xr_sem, zs_sem, zd_sem, zu_sem = sems
     rows = q.shape[2]
@@ -119,6 +119,9 @@
                     send(px.at[step - 1, zb, s], xr.at[slot, zb, s], xs_sem.at[step - 1, zb, s],
                          xr_sem.at[slot, zb, s], place.at(place.side(step), z))
 
+        if meanwhile is not None:
+            meanwhile(k)
+
         zc = place.outward(jnp.maximum(k - 1, 0))
 
         @pl.when((k > 0) & (zc < z))
@@ -139,6 +142,8 @@
                 send(sb.at[zc, s], zu.at[zc, s], zs_sem.at[zc, s], zu_sem.at[zc, s],
                      place.at(place.x, z + 1))
 
+    if meanwhile is not None:
+        meanwhile(None)
     for s in range(splits):
         sides(z, s)
         below(z, s)
@@ -156,16 +161,20 @@
 
 
 def front_kernel(
-    nx, nz, splits,
+    nx, nz, splits, blocks,
     hid, weight_in, residual, post_gain, final_gain, targets, vocab, bias,
-    normed_out, dlogits_out, stream_out, losses_out,
-    units, weight, px, xr, q, sb, zd, zu, normed,
-    targets_out, vocab_part, scores, exps, stats, stats_in, total_own, total_in,
-    xs_sem, xr_sem, zs_sem, zd_sem, zu_sem,
-    hid_send, hid_recv, tgt_send, tgt_recv,
-    side_send, line_send, gather_recv, core_send, core_recv, out_sem,
-    weight_sem, vocab_sem, stats_send, stats_recv, total_send, total_recv, grad_sem,
+    *refs,
 ):
+    normed_out, refs = refs[:blocks], refs[blocks:]
+    (
+        dlogits_out, stream_out, losses_out,
+        units, weight, px, xr, q, sb, zd, zu, normed,
+        targets_out, vocab_part, scores, exps, stats, stats_in, total_own, total_in,
+        xs_sem, xr_sem, zs_sem, zd_sem, zu_sem,
+        hid_send, hid_recv, tgt_send, tgt_recv,
+        side_send, line_send, gather_recv, core_send, core_recv, out_sem,
+        weight_sem, vocab_sem, stats_send, stats_recv, total_send, total_recv, grad_sem,
+    ) = refs
     place = Place(nx, nz)
     count, vp, z = place.count, place.vp, place.z
     split_rows, width = q.shape[2], q.shape[3]
@@ -234,7 +243,7 @@
 
         row_loop(split_rows, 16, norms)
 
-    blocks, block_width = normed_out.shape[0], normed_out.shape[-1]
+    block_width = width // blocks
     plane = place.dp // 2
 
     def keep(c, i, s):
@@ -243,7 +252,7 @@
             at = (there * 2 + lax.rem(core + b, 2)) * block_width
             pltpu.make_async_copy(
                 normed.at[c, i, s, :, pl.ds(pl.multiple_of(at, block_width), block_width)],
-                normed_out.at[b, c, i, s], out_sem.at[c, i, s],
+                normed_out[b].at[c, i, s], out_sem.at[c, i, s],
             ).start()
 
     def to_core(i, s):
@@ -460,15 +469,15 @@
     cols, lanes = bias.shape[1], targets.shape[1]
     flops = 2 * count * rows * weight.shape[0] * width
     return pl.pallas_call(
-        functools.partial(front_kernel, nx, nz, splits),
+        functools.partial(front_kernel, nx, nz, splits, blocks),
         out_shape=(
-            jax.ShapeDtypeStruct((blocks, 2, count, splits, split_rows, width // blocks), bf16),
+            *[jax.ShapeDtypeStruct((2, count, splits, split_rows, width // blocks), bf16)] * blocks,
             jax.ShapeDtypeStruct((2, count, rows, cols), bf16),
             jax.ShapeDtypeStruct((splits, split_rows, width), bf16),
             jax.ShapeDtypeStruct((1, lanes), f32),
         ),
         in_specs=[hbm] * 2 + [vmem] * 4 + [hbm, vmem],
-        out_specs=(hbm, hbm, vmem, vmem),
+        out_specs=(*[hbm] * blocks, hbm, vmem, vmem),
         scratch_shapes=[pltpu.VMEM(hid.shape, bf16), pltpu.VMEM(weight.shape, bf16)]
         + rs_scratch(nx, nz, splits, split_rows, width)
         + [
@@ -501,10 +510,11 @@
 
 def back_kernel(
     nx, nz, splits,
-    dlogits, vocab, own_out,
-    grads, vocab_part, terms, given, theirs, px, xr, q, sb, zd, zu,
+    dlogits, vocab, kept_rows, given_rows, own_out, kept_out, cross_out,
+    grads, vocab_part, token_rows, turned, kept, cross, terms, given, theirs, px, xr, q, sb, zd, zu,
     xs_sem, xr_sem, zs_sem, zd_sem, zu_sem,
     load_sem, vocab_sem, core_send, core_recv,
+    rows_sem, kept_sem, cross_send, cross_recv,
 ):
     place = Place(nx, nz)
     count, z = place.count, place.z
@@ -532,11 +542,47 @@
     def _(k):
         load(place.outward(k))
 
+    for b, ref in enumerate((kept_rows, given_rows)):
+        pltpu.make_async_copy(ref, token_rows.at[b], rows_sem.at[b]).start()
+
+    tokens, _ = token_rows.shape[1:]
+    slab = min(tokens, 256)
+    span = kept.shape[2]
+
+    def turn():
+        @pl.loop(1, nz)
+        def _(k):
+            for step in range(nx):
+                i = place.outward(k) * nx + place.side(step)
+                for c in range(2):
+                    arrived(grads.at[c, i], load_sem.at[c, i])
+
+        for b in range(2):
+            arrived(token_rows.at[b], rows_sem.at[b])
+
+            @pl.loop(0, tokens // slab)
+            def _(n):
+                at = pl.ds(pl.multiple_of(n * slab, slab), slab)
+                turned[b, :, at] = jnp.transpose(token_rows[b, at, :])
+
+    def own_gradient(k):
+        at = pl.ds(pl.multiple_of(k * span, span), span)
+        part = grads[:, :, :, at].reshape(tokens, span)
+        kept[k] = jnp.dot(turned[0], part, preferred_element_type=f32)
+        cross[k] = jnp.dot(turned[1], part, preferred_element_type=f32).astype(bf16)
+        pltpu.make_async_copy(kept.at[k], kept_out.at[:, at], kept_sem.at[k]).start()
+        send(cross.at[k], cross_out.at[:, at], cross_send.at[k], cross_recv.at[k],
+             (place.vp, place.other_core))
+
     def produce(zb):
         for step in range(nx):
             i = zb * nx + place.side(step)
-            for c in range(2):
-                arrived(grads.at[c, i], load_sem.at[c, i])
+
+            @pl.when(zb == 0)
+            def _():
+                for c in range(2):
+                    arrived(grads.at[c, i], load_sem.at[c, i])
+
             block = jnp.concatenate([grads[0, i], grads[1, i]], axis=0)
 
             @pl.loop(0, pieces)
@@ -572,14 +618,39 @@
 
                 row_loop(split_rows, 16, body)
 
+    count_own = kept.shape[0]
+
+    early = count_own // 2
+
+    def meanwhile(k):
+        if k is None:
+            pl.loop(early, count_own)(own_gradient)
+            return
+
+        @pl.when(k == 0)
+        def _():
+            turn()
+
+        if early > 0:
+            @pl.when(k == nz)
+            def _():
+                pl.loop(0, early)(own_gradient)
+
     line_reduce_scatter(
-        place, splits, produce, px, xr, q, sb, zd, zu, (xs_sem, xr_sem, zs_sem, zd_sem, zu_sem)
+        place, splits, produce, px, xr, q, sb, zd, zu, (xs_sem, xr_sem, zs_sem, zd_sem, zu_sem),
+        meanwhile,
     )
     for s in range(splits):
         def body(r):
             own_out[s, r] = q[z, s, r]
 
         row_loop(split_rows, 16, body)
+
+    @pl.loop(0, kept.shape[0])
+    def _(k):
+        arrived(kept.at[k], kept_sem.at[k])
+        arrived(cross.at[k], cross_send.at[k])
+        arrived(cross.at[k], cross_recv.at[k])
 
     @pl.loop(0, count)
     def _(i):
@@ -587,37 +658,48 @@
             arrived(given.at[i, s], core_send.at[i, s])
 
 
-def back(nx, nz, splits, dlogits, vocab):
+def back(nx, nz, splits, dlogits, vocab, kept_rows, given_rows):
     _, count, rows, cols = dlogits.shape
     width = vocab.shape[0]
     split_rows = rows // splits
     piece = math.gcd(width, 512)
+    tokens, block = kept_rows.shape
+    steps = max(1, min(nz, cols // 512))
     dma = pltpu.SemaphoreType.DMA
     shape = (count, splits, split_rows, width)
     hbm = pl.BlockSpec(memory_space=pl.ANY)
     return pl.pallas_call(
         functools.partial(back_kernel, nx, nz, splits),
-        out_shape=jax.ShapeDtypeStruct((splits, split_rows, width), f32),
-        in_specs=[hbm, hbm],
-        out_specs=pl.BlockSpec(memory_space=pltpu.VMEM),
+        out_shape=(
+            jax.ShapeDtypeStruct((splits, split_rows, width), f32),
+            jax.ShapeDtypeStruct((block, cols), f32),
+            jax.ShapeDtypeStruct((block, cols), bf16),
+        ),
+        in_specs=[hbm] * 4,
+        out_specs=(pl.BlockSpec(memory_space=pltpu.VMEM), hbm, hbm),
         scratch_shapes=[
             pltpu.VMEM((2, count, rows, cols), bf16),
             pltpu.VMEM((width // piece, piece, cols), bf16),
+            pltpu.VMEM((2, tokens, block), bf16),
+            pltpu.VMEM((2, block, tokens), bf16),
+            pltpu.VMEM((steps, block, cols // steps), f32),
+            pltpu.VMEM((steps, block, cols // steps), bf16),
             pltpu.VMEM((nx, splits, split_rows, width), f32),
             pltpu.VMEM(shape, bf16),
             pltpu.VMEM(shape, bf16),
         ]
         + rs_scratch(nx, nz, splits, split_rows, width)
         + rs_sems(nx, nz, splits)
-        + [dma((2, count)), dma((width // piece,)), dma((count, splits)), dma((count, splits))],
+        + [dma((2, count)), dma((width // piece,)), dma((count, splits)), dma((count, splits))]
+        + [dma((2,)), dma((steps,)), dma((steps,)), dma((steps,))],
         compiler_params=pltpu.CompilerParams(
-            collective_id=1, has_side_effects=True, vmem_limit_bytes=56 << 20
+            collective_id=1, has_side_effects=True, vmem_limit_bytes=62 << 20
         ),
         cost_estimate=pl.CostEstimate(
             flops=4 * count * rows * cols * width, bytes_accessed=1 << 24, transcendentals=0
         ),
         name="back",
-    )(dlogits, vocab)
+    )(dlogits, vocab, kept_rows, given_rows)
 
 
 def on_device(
@@ -634,17 +716,17 @@
     padded = jnp.pad(targets, (0, lanes - rows)).reshape(1, lanes)
     cols = vocab_matrix.shape[1] // 2
     bias_half = lax.dynamic_slice_in_dim(vocab_bias, core * cols, cols, 0)
-    normed, dlogits, stream, losses = front(
+    *normed, dlogits, stream, losses = front(
         nx, nz, splits, 2 * planes, units, down_weight, residual,
         post_gain.reshape(1, -1), final_gain.reshape(1, -1), padded,
         vocab_matrix, bias_half.reshape(1, -1),
     )
     stream = stream.reshape(rows, width)
     tokens = 2 * count * rows
-    token_rows = normed.reshape(2 * planes, tokens, width // (2 * planes))
+    block = width // (2 * planes)
+    token_rows = [part.reshape(tokens, block) for part in normed]
     dlogits_2d = dlogits.reshape(tokens, cols)
 
-    core_pairs = [(d, d ^ 1) for d in range(dp_size)]
     spans = column_spans(cols)
     arrivals = []
     source = dlogits_2d
@@ -662,17 +744,11 @@
                 ]
                 got.append(lax.ppermute(grads, "dp", to))
         arrivals.append(got)
-    dnormed = back(nx, nz, splits, source.reshape(dlogits.shape), vocab_matrix)
-    dnormed, source = lax.optimization_barrier((dnormed, source))
+    dnormed, kept, given = back(
+        nx, nz, splits, source.reshape(dlogits.shape), vocab_matrix,
+        token_rows[0], token_rows[1],
+    )
     dnormed = dnormed.reshape(rows, width)
-    halves = [
-        lax.dot_general(
-            token_rows[c], source, (((0,), (0,)), ((), ())), preferred_element_type=f32,
-        )
-        for c in (1, 0)
-    ]
-    given = lax.ppermute(halves[0].astype(bf16), "dp", core_pairs)
-    kept = halves[1]
 
     def total(c, base):
         parts = [

time: 382 us -> 288 us (0.75)
  waiting for transfers between devices: 86.6 us -> 1.99 us
  matrix products: 32.2 us -> 19.1 us
  local copies, waits for them, and re-layouts: 11.3 us -> 4.7 us
  other arithmetic: 5.75 us -> 12.1 us
    ppermute x4, waiting for transfers between devices: 86.6 us -> 1.99 us  [on_device(): got.append(lax.ppermute(grads, 'dp', to))]
    dot_general x2 -> x0, matrix products: 18.7 us -> none  [on_device(): lax.dot_general(token_rows[c], source, (((0,), (0,)), ((), ())), preferre...]
    dot_general x4, matrix products: 13.5 us -> 19.1 us  [on_device(): lax.dot_general(token_rows[2 * shift + c], source[:, low:high], (((0,), (...]
    slice x1 -> x0, local copies, waits for them, and re-layouts: 4.98 us -> none  [on_device(): token_rows[c]]
  transfers between devices with their start and end apart: 5 -> 4, of which waited for: 2 -> 1; matrix products, arithmetic and copies ran while one was open for 1% -> 2% of each run, Pallas kernels for 0% -> 29%
where the time goes in v1:
time: 288 us; the launch traced here: 285 us
  Pallas kernels  242 us (84%)
  matrix products  19.1 us (7%)
  other arithmetic  12.1 us (4%)
  local copies, waits for them, and re-layouts  4.7 us (2%)
  starting transfers between devices  3.97 us (1%)
    pallas_call x1, Pallas kernels, front(): pl.pallas_call(functools.partial(front_kernel, nx, nz, splits, blocks), o...  159 us
    pallas_call x1, Pallas kernels, back(): pl.pallas_call(functools.partial(back_kernel, nx, nz, splits), out_shape=...  83 us
    dot_general x4, matrix products, on_device(): lax.dot_general(token_rows[2 * shift + c], source[:, low:high], (((0,), (...  19.1 us
  transfers between devices with their start and end apart: 4, of which 1 were waited for; matrix products, arithmetic and copies ran while one was open for 2% of the time, Pallas kernels for 29%

profile of v1, /device:TPU:11, one launch (start us, length us, event | category | flops | bytes accessed | tf_op | source)
XLA Modules:
  0.0 284.9 jit_solution(17641013882618914525)
XLA Ops:
  0.6 0.0 copy-start.3
  0.7 1.8 copy.11
  2.5 1.6 copy.12
  4.1 0.0 copy-done.3
  4.1 0.6 dynamic_slice.3
  4.7 159.3 %front.1 = (bf16[2,8,4,32,512]{4,3,2,1,0:T(8,128)(2,1)}, bf16[2,8,4,32,512]{4,3,2,1,0:T(8,128)(2,1)}, bf16[2,8,4,32,512]{4,3,2,1,0:T(8,128)(2,1)}, bf16[2,8,4,32...) custom-call(bf16[8,128,704]{2,1,0:T(8,128)(2,1)} %bitcast.30, ...), custom_call_target="tpu_custom_call" | custom-call | flops 2952790016 | bytes 16777216 | tf_op jit(solution)/shard_map/front/pallas_call | solution.py:471
  163.9 0.0 copy-start.5
  163.9 0.0 copy-start.4
  163.9 4.5 %fusion.19 = bf16[512,512]{1,0:T(8,128)(2,1)} fusion(bf16[2048,512]{1,0:T(8,128)(2,1)} %bitcast.45, bf16[2048,2048]{1,0:T(8,128)(2,1)} %bitcast.37), kind=kOutput, calls=%fused_computation.18 | convolution fusion | flops 1074003968 | bytes 4718592 | tf_op jit(solution)/shard_map/dot_general | solution.py:737
  168.4 0.0 copy-done.5
  168.4 3.7 %fusion.16 = bf16[512,512]{1,0:T(8,128)(2,1)} fusion(bf16[2048,512]{1,0:T(8,128)(2,1)S(1)} %bitcast.43, bf16[2048,2048]{1,0:T(8,128)(2,1)} %bitcast.38), kind=kOutput, calls=%fused_computation.17 | convolution fusion | flops 1074003968 | bytes 4718592 | tf_op jit(solution)/shard_map/dot_general | solution.py:737
  172.2 0.0 copy-done.4
  172.2 6.3 %fusion.6 = bf16[512,1536]{1,0:T(8,128)(2,1)} fusion(bf16[2048,512]{1,0:T(8,128)(2,1)} %bitcast.46, bf16[2048,2048]{1,0:T(8,128)(2,1)S(1)} %bitcast.39), kind=kOutput, calls=%fused_computation.9 | convolution fusion | flops 3222011904 | bytes 9961472 | tf_op jit(solution)/shard_map/dot_general | solution.py:737
  178.4 4.6 %fusion.9 = bf16[512,1536]{1,0:T(8,128)(2,1)} fusion(bf16[2048,512]{1,0:T(8,128)(2,1)S(1)} %bitcast.44, bf16[2048,2048]{1,0:T(8,128)(2,1)S(1)} %bitcast.40), kind=kOutput, calls=%fused_computation.10 | convolution fusion | flops 3222011904 | bytes 9961472 | tf_op jit(solution)/shard_map/dot_general | solution.py:737
  183.1 2.2 collective-permute-start.3
  185.3 0.1 collective-permute-start.1
  185.5 1.0 collective-permute-start.2
  186.4 0.6 collective-permute-start
  187.1 0.0 copy-start
  187.1 0.0 copy-start.2
  187.1 83.0 %back.1 = (f32[4,32,2048]{2,1,0:T(8,128)}, f32[512,2048]{1,0:T(8,128)}, bf16[512,2048]{1,0:T(8,128)(2,1)}) custom-call(bf16[2,8,128,2048]{3,2,1,0:T(8,128)(2,1)} %get-tuple-element.25, bf16[2048,4096]{1,0:T(8,128)(2,1)} %vocab.3, bf16[2048,512]{1,0:T(8,128)(2,1)} %bitcast.41, bf16[2048,512]{1,0:T(8,128)(2,1)} %bitcast.42), custom_call_target="tpu_custom_call" | custom-call | flops 17179869184 | bytes 16777216 | tf_op jit(solution)/shard_map/back/pallas_call | solution.py:671
  270.0 0.0 copy-done
  270.1 0.2 multiply_reduce_fusion.1
  270.2 0.0 copy-done.2
  270.2 1.5 multiply_reduce_fusion
  271.8 0.1 rsqrt.13
  271.9 0.1 div.10
  272.0 0.0 copy-start.1
  272.0 2.7 fusion.24
  274.6 0.0 collective-permute-done.2
  274.7 2.0 collective-permute-done
  276.6 0.0 collective-permute-done.3
  276.6 0.0 collective-permute-done.1
  276.6 0.0 copy-done.1
  276.6 3.8 %fusion.5 = (f32[512,2048]{1,0:T(8,128)S(1)}, f32[512,2048]{1,0:T(8,128)S(1)}) fusion(bf16[512,2048]{1,0:T(8,128)(2,1)S(1)} %copy-done.1, f32[512,2048]{1,0:T(8,128)} %get-tuple-element.33, pred[]{:T(512)S(6)} %eq.6, bf16[512,1536]{1,0:T(8,128)(2,1)} %collective-permute-done.3, bf16[512,512]{1,0:T(8,128)(2,1)S(1)} %collective-permute-done.2, ...), kind=kLoop, calls=%fused_computation.8 | loop fusion | flops 13631488 | bytes 18874368 | tf_op jit(solution)/shard_map/jit(_where)/select_n | solution.py:762
  280.4 0.0 copy-start.6
  280.4 3.9 %pad_maximum_fusion = f32[512,4096]{1,0:T(8,128)} fusion(f32[512,2048]{1,0:T(8,128)S(1)} %get-tuple-element.40, f32[512,2048]{1,0:T(8,128)S(1)} %get-tuple-element.39), kind=kLoop, calls=%fused_computation | loop fusion | flops 2097152 | bytes 16777216 | tf_op jit(solution)/shard_map/concatenate | solution.py:761
  284.4 0.0 copy-done.6
  284.4 0.5 copy.14
  (2 shorter events, 0.0 us)
Async XLA Ops:
  0.6 3.4 %copy-start.3 = (f32[4096]{0:T(1024)S(1)}, f32[4096]{0:T(1024)}, u32[]{:S(2)}) copy-start(f32[4096]{0:T(1024)} %param.14) | copy-start | bytes 49156
  163.9 4.5 %copy-start.5 = (bf16[2,8,4,32,512]{4,3,2,1,0:T(8,128)(2,1)S(1)}, bf16[2,8,4,32,512]{4,3,2,1,0:T(8,128)(2,1)}, u32[]{:S(2)}) copy-start(bf16[2,8,4,32,512]{4,3,2,1,0:T(8,128)(2,1)} %get-tuple-element.23) | copy-start | bytes 6291460
  163.9 8.2 %copy-start.4 = (bf16[2,8,128,2048]{3,2,1,0:T(8,128)(2,1)S(1)}, bf16[2,8,128,2048]{3,2,1,0:T(8,128)(2,1)}, u32[]{:S(2)}) copy-start(bf16[2,8,128,2048]{3,2,1,0:T(8,128)(2,1)} %get-tuple-element.25) | copy-start | bytes 25165828
  183.1 93.5 %collective-permute-start.3 = (bf16[512,1536]{1,0:T(8,128)(2,1)}, bf16[512,1536]{1,0:T(8,128)(2,1)}, u32[]{:S(2)}, u32[]{:S(2)}) collective-permute-start(bf16[512,1536]{1,0:T(8,128)(2,1)} %fusion.9), channel_id=1, source_target_pairs={{0,3},{1,2},{2,1},{3,0},{4,7},{5,6},{6,5},{7,4},{8,11},{9,10},{10,... | collective-permute-start | bytes 4718600 | tf_op jit(solution)/shard_map/ppermute | solution.py:745
  185.3 91.3 %collective-permute-start.1 = (bf16[512,1536]{1,0:T(8,128)(2,1)}, bf16[512,1536]{1,0:T(8,128)(2,1)}, u32[]{:S(2)}, u32[]{:S(2)}) collective-permute-start(bf16[512,1536]{1,0:T(8,128)(2,1)} %fusion.6), channel_id=1, source_target_pairs={{0,2},{1,3},{2,0},{3,1},{4,6},{5,7},{6,4},{7,5},{8,10},{9,11},{10,... | collective-permute-start | bytes 4718600 | tf_op jit(solution)/shard_map/ppermute | solution.py:745
  185.5 89.2 %collective-permute-start.2 = (bf16[512,512]{1,0:T(8,128)(2,1)}, bf16[512,512]{1,0:T(8,128)(2,1)S(1)}, u32[]{:S(2)}, u32[]{:S(2)}) collective-permute-start(bf16[512,512]{1,0:T(8,128)(2,1)} %fusion.16), channel_id=1, source_target_pairs={{0,3},{1,2},{2,1},{3,0},{4,7},{5,6},{6,5},{7,4},{8,11},{9,10},{10,... | collective-permute-start | bytes 1572872 | tf_op jit(solution)/shard_map/ppermute | solution.py:745
  186.4 90.2 %collective-permute-start = (bf16[512,512]{1,0:T(8,128)(2,1)}, bf16[512,512]{1,0:T(8,128)(2,1)S(1)}, u32[]{:S(2)}, u32[]{:S(2)}) collective-permute-start(bf16[512,512]{1,0:T(8,128)(2,1)} %fusion.19), channel_id=1, source_target_pairs={{0,2},{1,3},{2,0},{3,1},{4,6},{5,7},{6,4},{7,5},{8,10},{9,11},{10,... | collective-permute-start | bytes 1572872 | tf_op jit(solution)/shard_map/ppermute | solution.py:745
  187.1 83.0 %copy-start = (bf16[4,32,2048]{2,1,0:T(8,128)(2,1)S(1)}, bf16[4,32,2048]{2,1,0:T(8,128)(2,1)}, u32[]{:S(2)}) copy-start(bf16[4,32,2048]{2,1,0:T(8,128)(2,1)} %get-tuple-element.22) | copy-start | bytes 1572868
  187.1 83.2 %copy-start.2 = (f32[2048]{0:T(1024)S(1)}, f32[2048]{0:T(1024)}, u32[]{:S(2)}) copy-start(f32[2048]{0:T(1024)} %param.12) | copy-start | bytes 24580
  272.0 4.7 %copy-start.1 = (bf16[512,2048]{1,0:T(8,128)(2,1)S(1)}, bf16[512,2048]{1,0:T(8,128)(2,1)}, u32[]{:S(2)}) copy-start(bf16[512,2048]{1,0:T(8,128)(2,1)} %get-tuple-element.36) | copy-start | bytes 6291460
  280.4 4.0 %copy-start.6 = (f32[1,128]{1,0:T(1,128)S(1)}, f32[1,128]{1,0:T(1,128)}, u32[]{:S(2)}) copy-start(f32[1,128]{1,0:T(1,128)} %get-tuple-element.21) | copy-start | bytes 1540
